TPU v7x, 32 devices: a whole 2x2x4 slice. The times are simulated.
32 devices in a mesh: ep: 8 (over z, x), tp: 4 (over y, core).
Axes of the slice: x: 2, y: 2, z: 4, core: 2. Of those that a mesh axis runs over, the one named last changes fastest.
Arguments:
- tokens: bfloat16 [1536, 2048], P('ep'), may hold values from -6 to 6
- cotangent: bfloat16 [1536, 2048], P('ep'), may hold values from -6 to 6
- routing: int32 [1536, 2], P('ep'), may hold values from 0 to 7, all different within a row; in each aligned block of 192 rows (0 to 191, 192 to 383, ...) at most 60 rows name the same one
- route_weights: float32 [1536, 2], P('ep'), may hold values from 0.1 to 1
- w_gate: bfloat16 [8, 2048, 2048], P('ep', None, 'tp'), may hold values from -0.125 to 0.125
- w_up: bfloat16 [8, 2048, 2048], P('ep', None, 'tp'), may hold values from -0.125 to 0.125
- w_down: bfloat16 [8, 2048, 2048], P('ep', 'tp'), may hold values from -0.125 to 0.125
Outputs:
- grad_tokens: bfloat16 [1536, 2048], P('ep')
- grad_weights: bfloat16 [1536, 2], P('ep')
- grad_gate: bfloat16 [8, 2048, 2048], P('ep', None, 'tp')
- grad_up: bfloat16 [8, 2048, 2048], P('ep', None, 'tp')
- grad_down: bfloat16 [8, 2048, 2048], P('ep', 'tp')
Inputs may be any that keep to these rules, and one draw needn't show every extreme that they name: `routing`: each row names 2 different experts. Within the rows of one device no expert is named more than 60 times, and in every draw some expert is named exactly 60 times by some device's rows.
All inputs are finite; a program needn't handle non-finite values.
Results may differ from a plain program's by a relative error of at most 0.019.
Values may be sent and summed in bfloat16 or wider, within the bound.
A program may use at most 64 MiB of HBM per device.

v0:
```python
import jax
import jax.numpy as jnp
from jax import lax
from jax.sharding import PartitionSpec as P


def slot_tables(routing, experts, capacity):
    flat = routing.reshape(-1)
    onehot = (flat[:, None] == jnp.arange(experts, dtype=jnp.int32)[None, :]).astype(jnp.int32)
    before = jnp.cumsum(onehot, axis=0) - onehot
    within = jnp.sum(before * onehot, axis=1)
    target = flat * capacity + within
    chosen = jnp.arange(experts * capacity, dtype=jnp.int32)[:, None] == target[None, :]
    return (target, chosen)


def on_device(tokens, cotangent, routing, route_weights, w_gate, w_up, w_down):
    experts = lax.axis_size("ep")
    local_tokens, top_count = routing.shape
    width = tokens.shape[1]
    capacity = max(2, (5 * local_tokens * top_count + 4 * experts - 1) // (4 * experts))
    slot_total = experts * capacity
    target, chosen = slot_tables(routing, experts, capacity)
    picked = chosen.reshape(slot_total, local_tokens, top_count).astype(jnp.float32)
    by_token = jnp.sum(picked, axis=2).astype(jnp.bfloat16)
    slot_weight = jnp.sum(picked * route_weights[None, :, :], axis=(1, 2)).astype(jnp.bfloat16)
    send_rows = jnp.dot(by_token, tokens, preferred_element_type=jnp.float32).astype(jnp.bfloat16)
    send_back = jnp.dot(by_token, cotangent, preferred_element_type=jnp.float32).astype(
        jnp.bfloat16
    )
    rows_in, weight_in = (
        lax.all_to_all(
            send_rows.reshape(experts, capacity, width),
            "ep",
            split_axis=0,
            concat_axis=0,
            tiled=True,
        ),
        lax.all_to_all(
            slot_weight.reshape(experts, capacity), "ep", split_axis=0, concat_axis=0, tiled=True
        ),
    )
    back_in = lax.all_to_all(
        send_back.reshape(experts, capacity, width), "ep", split_axis=0, concat_axis=0, tiled=True
    )
    rows = rows_in.reshape(slot_total, width)
    back = back_in.reshape(slot_total, width)
    weight = weight_in.reshape(slot_total, 1).astype(jnp.float32)
    wgate = w_gate[0]
    wup = w_up[0]
    wdown = w_down[0]
    pre_gate = jnp.dot(rows, wgate, preferred_element_type=jnp.float32)
    pre_up = jnp.dot(rows, wup, preferred_element_type=jnp.float32)
    along = jnp.einsum("rd,fd->rf", back, wdown, preferred_element_type=jnp.float32)
    gate_sig = jax.nn.sigmoid(pre_gate)
    gate_act = pre_gate * gate_sig
    hidden = gate_act * pre_up
    hidden_grad = weight * along
    gate_grad = (hidden_grad * pre_up * gate_sig * (1.0 + pre_gate * (1.0 - gate_sig))).astype(
        jnp.bfloat16
    )
    up_grad = (hidden_grad * gate_act).astype(jnp.bfloat16)
    scaled = (weight * hidden).astype(jnp.bfloat16)
    grad_gate = jnp.einsum("rd,rf->df", rows, gate_grad, preferred_element_type=jnp.float32).astype(
        jnp.bfloat16
    )
    grad_up = jnp.einsum("rd,rf->df", rows, up_grad, preferred_element_type=jnp.float32).astype(
        jnp.bfloat16
    )
    grad_down = jnp.einsum("rf,rd->fd", scaled, back, preferred_element_type=jnp.float32).astype(
        jnp.bfloat16
    )
    row_part = jnp.einsum(
        "rf,df->rd", gate_grad, wgate, preferred_element_type=jnp.float32
    ) + jnp.einsum("rf,df->rd", up_grad, wup, preferred_element_type=jnp.float32)
    slot_part = jnp.sum(hidden * along, axis=1)
    row_share = lax.psum_scatter(
        row_part.reshape(experts, capacity, width).astype(jnp.bfloat16),
        "tp",
        scatter_dimension=2,
        tiled=True,
    )
    slot_sum = lax.psum(slot_part.astype(jnp.bfloat16), "tp")
    back_grad = slot_sum.reshape(experts, capacity)
    home_rows, home_grad = (
        lax.all_to_all(row_share, "ep", split_axis=0, concat_axis=0, tiled=True),
        lax.all_to_all(back_grad, "ep", split_axis=0, concat_axis=0, tiled=True),
    )
    feature_part = jnp.einsum(
        "st,sd->td",
        by_token,
        home_rows.reshape(slot_total, home_rows.shape[2]),
        preferred_element_type=jnp.float32,
    ).astype(jnp.bfloat16)
    grad_tokens = lax.all_gather(feature_part, "tp", axis=1, tiled=True)
    grad_weights = home_grad.reshape(-1)[target].reshape(local_tokens, top_count)
    return (grad_tokens, grad_weights, grad_gate[None], grad_up[None], grad_down[None])


def solution(mesh):
    return jax.shard_map(
        on_device,
        mesh=mesh,
        in_specs=(
            P("ep", None),
            P("ep", None),
            P("ep", None),
            P("ep", None),
            P("ep", None, "tp"),
            P("ep", None, "tp"),
            P("ep", "tp", None),
        ),
        out_specs=(
            P("ep", None),
            P("ep", None),
            P("ep", None, "tp"),
            P("ep", None, "tp"),
            P("ep", "tp", None),
        ),
        check_vma=False,
    )
```

profile of v0, /device:TPU:0, one launch (start us, length us, event | category | flops | bytes accessed | tf_op | source)
XLA Modules:
  0.0 210.8 jit_solution(13199292134892144586)
XLA Ops:
  7.2 0.9 copy.26
  8.4 0.9 reduce-window.6
  9.9 0.9 select_reduce_fusion
  11.5 7.3 %all-to-all-start = ((bf16[8,1,60]{2,1,0:T(2,128)(2,1)}), bf16[8,1,60]{2,1,0:T(2,128)(2,1)S(1)}, u32[]{:S(2)}, u32[]{:S(2)}) async-start(bf16[8,1,60]{2,1,0:T(2,128)(2,1)} %convert_element_type.95), calls=%async_computation | async-start | bytes 8192 | tf_op jit(solution)/shard_map/all_to_all | solution.py:39
  18.8 3.1 %convolution_convert_fusion.3 = bf16[480,2048]{1,0:T(8,128)(2,1)} fusion(bf16[192,2048]{1,0:T(8,128)(2,1)} %param.7, bf16[480,192]{0,1:T(8,128)(2,1)S(1)} %get-tuple-element.21), kind=kOutput, calls=%fused_computation.5 | convolution fusion | flops 378470400 | bytes 2936832 | tf_op jit(solution)/shard_map/dot_general | solution.py:27
  21.9 2.7 %reshape.131 = bf16[8,60,2048]{2,1,0:T(8,128)(2,1)} reshape(bf16[480,2048]{1,0:T(8,128)(2,1)} %convolution_convert_fusion.3) | data formatting | bytes 3932160 | tf_op jit(solution)/shard_map/reshape | solution.py:33
  25.2 5.5 %all-to-all-start.2 = ((bf16[8,60,2048]{2,1,0:T(8,128)(2,1)}), bf16[8,60,2048]{2,1,0:T(8,128)(2,1)}, u32[]{:S(2)}, u32[]{:S(2)}) async-start(bf16[8,60,2048]{2,1,0:T(8,128)(2,1)} %reshape.131), calls=%async_computation.2 | async-start | bytes 4194304 | tf_op jit(solution)/shard_map/all_to_all | solution.py:32
  30.8 2.0 convolution_convert_fusion.4
  32.8 2.7 %reshape.129 = bf16[8,60,2048]{2,1,0:T(8,128)(2,1)} reshape(bf16[480,2048]{1,0:T(8,128)(2,1)} %convolution_convert_fusion.4) | data formatting | bytes 3932160 | tf_op jit(solution)/shard_map/reshape | solution.py:44
  35.5 43.1 %all-to-all-done.2 = bf16[8,60,2048]{2,1,0:T(8,128)(2,1)} async-done(((bf16[8,60,2048]{2,1,0:T(8,128)(2,1)}), bf16[8,60,2048]{2,1,0:T(8,128)(2,1)}, u32[]{:S(2)}, u32[]{:S(2)}) %all-to-all-start.2) | async-done | bytes 1966112 | tf_op jit(solution)/shard_map/all_to_all | solution.py:32
  78.5 4.3 %all-to-all-start.1 = ((bf16[8,60,2048]{2,1,0:T(8,128)(2,1)}), bf16[8,60,2048]{2,1,0:T(8,128)(2,1)}, u32[]{:S(2)}, u32[]{:S(2)}) async-start(bf16[8,60,2048]{2,1,0:T(8,128)(2,1)} %reshape.129), calls=%async_computation.1 | async-start | bytes 4194304 | tf_op jit(solution)/shard_map/all_to_all | solution.py:43
  83.0 2.7 %reshape.132 = bf16[480,2048]{1,0:T(8,128)(2,1)} reshape(bf16[8,60,2048]{2,1,0:T(8,128)(2,1)} %all-to-all-done.2) | data formatting | bytes 3932160 | tf_op jit(solution)/shard_map/reshape | solution.py:46
  85.8 3.8 %fusion.5 = f32[480,512]{1,0:T(8,128)} fusion(bf16[480,2048]{1,0:T(8,128)(2,1)} %reshape.132, bf16[1,2048,512]{2,1,0:T(8,128)(2,1)S(1)} %copy-done), kind=kOutput, calls=%fused_computation.12 | convolution fusion | flops 1006632960 | bytes 5046272 | tf_op jit(solution)/shard_map/dot_general | solution.py:52
  89.6 2.1 %fusion.8 = f32[480,512]{1,0:T(8,128)} fusion(bf16[480,2048]{1,0:T(8,128)(2,1)S(1)} %copy-done.3, bf16[1,2048,512]{2,1,0:T(8,128)(2,1)S(1)} %copy-done.1), kind=kOutput, calls=%fused_computation.15 | convolution fusion | flops 1006632960 | bytes 5046272 | tf_op jit(solution)/shard_map/dot_general | solution.py:53
  91.7 39.0 %all-to-all-done.1 = bf16[8,60,2048]{2,1,0:T(8,128)(2,1)} async-done(((bf16[8,60,2048]{2,1,0:T(8,128)(2,1)}), bf16[8,60,2048]{2,1,0:T(8,128)(2,1)}, u32[]{:S(2)}, u32[]{:S(2)}) %all-to-all-start.1) | async-done | bytes 1966112 | tf_op jit(solution)/shard_map/all_to_all | solution.py:43
  130.7 2.7 %reshape.130 = bf16[480,2048]{1,0:T(8,128)(2,1)} reshape(bf16[8,60,2048]{2,1,0:T(8,128)(2,1)} %all-to-all-done.1) | data formatting | bytes 3932160 | tf_op jit(solution)/shard_map/reshape | solution.py:47
  133.4 4.4 %multiply_reduce_fusion = (bf16[480]{0:T(512)(128)(2,1)S(1)}, bf16[480,512]{1,0:T(8,128)(2,1)S(1)}, bf16[480,512]{1,0:T(8,128)(2,1)S(1)}) fusion(f32[480,512]{1,0:T(8,128)} %fusion.8, f32[480,512]{1,0:T(8,128)} %fusion.5, f32[480]{0:T(512)S(1)} %reshape.136, bf16[480,2048]{1,0:T(8,128)(2,1)} %reshape.130, bf16[1,512,2048]{2,1,0:T(8,128)(2,1)} %param.13), kind=kOutput, calls=%fused_computation.21 | convolution fusion | flops 1010810368 | bytes 7015232 | tf_op jit(solution)/shard_map/rd,fd->rf/dot_general | solution.py:54
  137.8 1.2 fusion.3
  139.6 2.5 %add_convert_fusion = bf16[480,2048]{1,0:T(8,128)(2,1)} fusion(f32[480,2048]{1,0:T(8,128)S(1)} %fusion.3, bf16[480,512]{1,0:T(8,128)(2,1)S(1)} %get-tuple-element.24, bf16[1,2048,512]{2,1,0:T(8,128)(2,1)S(1)} %copy-done.2), kind=kOutput, calls=%fused_computation.1 | convolution fusion | flops 1008599040 | bytes 8486912 | tf_op jit(solution)/shard_map/rf,df->rd/dot_general | solution.py:75
  142.1 2.7 %convert_element_type.87 = bf16[8,60,2048]{2,1,0:T(8,128)(2,1)} reshape(bf16[480,2048]{1,0:T(8,128)(2,1)} %add_convert_fusion) | data formatting | bytes 3932160 | tf_op jit(solution)/shard_map/convert_element_type | solution.py:78
  145.1 5.7 %psum.7 = bf16[8,1,60]{2,0,1:T(8,128)(2,1)S(1)} all-reduce(bf16[8,1,60]{2,0,1:T(8,128)(2,1)S(1)} %all_to_all.23), channel_id=1, replica_groups=mesh['ep'=8,'tp'=4] {'tp'}, use_global_device_ids=true, to_apply=%region_7.8 | all-reduce | flops 480 | bytes 1920 | tf_op jit(solution)/shard_map/psum | solution.py:83
  151.4 4.9 %all-to-all-start.4 = ((bf16[8,1,60]{2,1,0:T(2,128)(2,1)}), bf16[8,1,60]{2,1,0:T(2,128)(2,1)S(1)}, u32[]{:S(2)}, u32[]{:S(2)}) async-start(bf16[8,1,60]{2,1,0:T(2,128)(2,1)} %copy.31), calls=%async_computation.5 | async-start | bytes 8192 | tf_op jit(solution)/shard_map/all_to_all | solution.py:87
  156.2 6.4 %all-to-all-done.4 = bf16[8,1,60]{2,1,0:T(2,128)(2,1)S(1)} async-done(((bf16[8,1,60]{2,1,0:T(2,128)(2,1)}), bf16[8,1,60]{2,1,0:T(2,128)(2,1)S(1)}, u32[]{:S(2)}, u32[]{:S(2)}) %all-to-all-start.4) | async-done | bytes 992 | tf_op jit(solution)/shard_map/all_to_all | solution.py:87
  162.6 12.6 %reduce-scatter.2.cloned.1.call-done = bf16[8,60,512]{2,1,0:T(8,128)(2,1)} async-done(((bf16[8,60,2048]{2,1,0:T(8,128)(2,1)}), bf16[8,60,512]{2,1,0:T(8,128)(2,1)}) %reduce-scatter.2.cloned.1.call-update) | async-done | bytes 491536 | tf_op jit(solution)/shard_map/reduce_scatter | solution.py:77
  175.2 5.5 %all-to-all-start.3 = ((bf16[8,60,512]{2,1,0:T(8,128)(2,1)}), bf16[8,60,512]{2,1,0:T(8,128)(2,1)S(1)}, u32[]{:S(2)}, u32[]{:S(2)}) async-start(bf16[8,60,512]{2,1,0:T(8,128)(2,1)} %reduce-scatter.2.cloned.1.call-done), calls=%async_computation.4 | async-start | bytes 1048576 | tf_op jit(solution)/shard_map/all_to_all | solution.py:86
  180.8 4.3 %fusion = bf16[1,2048,512]{2,1,0:T(8,128)(2,1)} fusion(bf16[480,2048]{1,0:T(8,128)(2,1)} %reshape.132, bf16[480,512]{1,0:T(8,128)(2,1)S(1)} %get-tuple-element.23), kind=kOutput, calls=%fused_computation.7 | convolution fusion | flops 1007681536 | bytes 4554752 | tf_op jit(solution)/shard_map/rd,rf->df/dot_general | solution.py:64
  185.1 2.6 %fusion.1 = bf16[1,2048,512]{2,1,0:T(8,128)(2,1)} fusion(bf16[480,2048]{1,0:T(8,128)(2,1)S(1)} %copy-done.4, bf16[480,512]{1,0:T(8,128)(2,1)S(1)} %copy-done.8), kind=kOutput, calls=%fused_computation.8 | convolution fusion | flops 1007681536 | bytes 4554752 | tf_op jit(solution)/shard_map/rd,rf->df/dot_general | solution.py:67
  187.8 2.8 %fusion.2 = bf16[1,512,2048]{2,1,0:T(8,128)(2,1)} fusion(bf16[480,2048]{1,0:T(8,128)(2,1)S(1)} %copy-done.5, f32[480]{0:T(512)S(1)} %reshape.136, f32[480,512]{1,0:T(8,128)S(1)} %copy-done.10, f32[480,512]{1,0:T(8,128)S(1)} %copy-done.9), kind=kOutput, calls=%fused_computation.9 | convolution fusion | flops 1009401856 | bytes 6031232 | tf_op jit(solution)/shard_map/rf,rd->fd/dot_general | solution.py:70
  190.7 2.8 %gather_fusion = bf16[384]{0:T(512)(128)(2,1)S(1)} fusion(bf16[480]{0:T(512)(128)(2,1)S(1)} %reshape.134, s32[1024]{0:T(1024)S(1)} %pad_clamp_fusion), kind=kCustom, calls=%fused_computation | custom fusion | bytes 3072 | tf_op jit(solution)/shard_map/gather | solution.py:96
  194.3 0.8 all-to-all-done.3
  195.4 7.7 %all_gather.3 = bf16[192,2048]{1,0:T(8,128)(2,1)S(1)} all-gather(bf16[192,512]{1,0:T(8,128)(2,1)S(1)} %convolution_convert_fusion.5), channel_id=1, replica_groups=mesh['ep'=8,'tp'=4] {'tp'}, dimensions={1}, use_global_device_ids=true | all-gather | bytes 983040 | tf_op jit(solution)/shard_map/all_gather | solution.py:95
  203.1 0.9 copy.34
  (48 shorter events, 5.0 us)
Async XLA Ops:
  7.2 78.6 %copy-start = (bf16[1,2048,512]{2,1,0:T(8,128)(2,1)S(1)}, bf16[1,2048,512]{2,1,0:T(8,128)(2,1)}, u32[]{:S(2)}) copy-start(bf16[1,2048,512]{2,1,0:T(8,128)(2,1)} %param.11) | copy-start | bytes 6291460
  11.5 13.7 %all-to-all-start = ((bf16[8,1,60]{2,1,0:T(2,128)(2,1)}), bf16[8,1,60]{2,1,0:T(2,128)(2,1)S(1)}, u32[]{:S(2)}, u32[]{:S(2)}) async-start(bf16[8,1,60]{2,1,0:T(2,128)(2,1)} %convert_element_type.95), calls=%async_computation | async-start | bytes 8192 | tf_op jit(solution)/shard_map/all_to_all | solution.py:39
  24.6 6.1 %copy-start.6 = (bf16[192,2048]{1,0:T(8,128)(2,1)S(1)}, bf16[192,2048]{1,0:T(8,128)(2,1)}, u32[]{:S(2)}) copy-start(bf16[192,2048]{1,0:T(8,128)(2,1)} %param.8) | copy-start | bytes 2359300
  25.2 53.3 %all-to-all-start.2 = ((bf16[8,60,2048]{2,1,0:T(8,128)(2,1)}), bf16[8,60,2048]{2,1,0:T(8,128)(2,1)}, u32[]{:S(2)}, u32[]{:S(2)}) async-start(bf16[8,60,2048]{2,1,0:T(8,128)(2,1)} %reshape.131), calls=%async_computation.2 | async-start | bytes 4194304 | tf_op jit(solution)/shard_map/all_to_all | solution.py:32
  78.5 52.2 %all-to-all-start.1 = ((bf16[8,60,2048]{2,1,0:T(8,128)(2,1)}), bf16[8,60,2048]{2,1,0:T(8,128)(2,1)}, u32[]{:S(2)}, u32[]{:S(2)}) async-start(bf16[8,60,2048]{2,1,0:T(8,128)(2,1)} %reshape.129), calls=%async_computation.1 | async-start | bytes 4194304 | tf_op jit(solution)/shard_map/all_to_all | solution.py:43
  82.9 92.3 %reduce-scatter.2.cloned.1.call-start = ((), (), s32[]{:S(2)}) async-start(), calls=%async_computation.6 | async-start | bytes 2621440 | tf_op jit(solution)/shard_map/reduce_scatter | solution.py:77
  85.8 3.8 %copy-start.1 = (bf16[1,2048,512]{2,1,0:T(8,128)(2,1)S(1)}, bf16[1,2048,512]{2,1,0:T(8,128)(2,1)}, u32[]{:S(2)}) copy-start(bf16[1,2048,512]{2,1,0:T(8,128)(2,1)} %param.12) | copy-start | bytes 6291460
  85.8 3.8 %copy-start.3 = (bf16[480,2048]{1,0:T(8,128)(2,1)S(1)}, bf16[480,2048]{1,0:T(8,128)(2,1)}, u32[]{:S(2)}) copy-start(bf16[480,2048]{1,0:T(8,128)(2,1)} %reshape.132) | copy-start | bytes 5898244
  137.8 1.3 copy-start.7
  137.8 1.8 copy-start.2
  151.4 11.3 %all-to-all-start.4 = ((bf16[8,1,60]{2,1,0:T(2,128)(2,1)}), bf16[8,1,60]{2,1,0:T(2,128)(2,1)S(1)}, u32[]{:S(2)}, u32[]{:S(2)}) async-start(bf16[8,1,60]{2,1,0:T(2,128)(2,1)} %copy.31), calls=%async_computation.5 | async-start | bytes 8192 | tf_op jit(solution)/shard_map/all_to_all | solution.py:87
  175.2 19.8 %all-to-all-start.3 = ((bf16[8,60,512]{2,1,0:T(8,128)(2,1)}), bf16[8,60,512]{2,1,0:T(8,128)(2,1)S(1)}, u32[]{:S(2)}, u32[]{:S(2)}) async-start(bf16[8,60,512]{2,1,0:T(8,128)(2,1)} %reduce-scatter.2.cloned.1.call-done), calls=%async_computation.4 | async-start | bytes 1048576 | tf_op jit(solution)/shard_map/all_to_all | solution.py:86
  180.7 4.4 %copy-start.4 = (bf16[480,2048]{1,0:T(8,128)(2,1)S(1)}, bf16[480,2048]{1,0:T(8,128)(2,1)}, u32[]{:S(2)}) copy-start(bf16[480,2048]{1,0:T(8,128)(2,1)} %reshape.132) | copy-start | bytes 5898244
  180.7 4.4 %copy-start.8 = (bf16[480,512]{1,0:T(8,128)(2,1)S(1)}, bf16[480,512]{1,0:T(8,128)(2,1)}, u32[]{:S(2)}) copy-start(bf16[480,512]{1,0:T(8,128)(2,1)} %copy-done.7) | copy-start | bytes 1474564
  185.1 2.7 %copy-start.5 = (bf16[480,2048]{1,0:T(8,128)(2,1)S(1)}, bf16[480,2048]{1,0:T(8,128)(2,1)}, u32[]{:S(2)}) copy-start(bf16[480,2048]{1,0:T(8,128)(2,1)} %reshape.130) | copy-start | bytes 5898244
  185.1 2.7 %copy-start.9 = (f32[480,512]{1,0:T(8,128)S(1)}, f32[480,512]{1,0:T(8,128)}, u32[]{:S(2)}) copy-start(f32[480,512]{1,0:T(8,128)} %fusion.5) | copy-start | bytes 2949124
  185.1 2.7 %copy-start.10 = (f32[480,512]{1,0:T(8,128)S(1)}, f32[480,512]{1,0:T(8,128)}, u32[]{:S(2)}) copy-start(f32[480,512]{1,0:T(8,128)} %fusion.8) | copy-start | bytes 2949124
Sparse Core Ops, SparseCore 0:
  145.0 30.2 reduce-scatter.1
where the time goes:
time: 212 us; the launch traced here: 211 us
  waiting for transfers between devices  102 us (48%)
  matrix products  29.2 us (14%)
  starting transfers between devices  27.6 us (13%)
  local copies, waits for them, and re-layouts  22 us (10%)
  between operations  14.2 us (7%)
  blocking collectives  13.3 us (6%)
    all_to_all x1, waiting for transfers between devices, on_device(): lax.all_to_all(send_rows.reshape(experts, capacity, width), 'ep', split_a...  43.1 us
    all_to_all x1, waiting for transfers between devices, on_device(): lax.all_to_all(send_back.reshape(experts, capacity, width), 'ep', split_a...  39 us
    reduce_scatter x1, waiting for transfers between devices, on_device(): lax.psum_scatter(row_part.reshape(experts, capacity, width).astype(jnp.bf...  12.6 us
    all_gather x1, blocking collectives, on_device(): grad_tokens = lax.all_gather(feature_part, 'tp', axis=1, tiled=True)  7.65 us
    all_to_all x1, starting transfers between devices, on_device(): lax.all_to_all(slot_weight.reshape(experts, capacity), 'ep', split_axis=0...  7.28 us
    all_to_all x1, waiting for transfers between devices, on_device(): lax.all_to_all(back_grad, 'ep', split_axis=0, concat_axis=0, tiled=True)  6.41 us
    psum x1, blocking collectives, on_device(): slot_sum = lax.psum(slot_part.astype(jnp.bfloat16), 'tp')  5.65 us
    all_to_all x1, starting transfers between devices, on_device(): lax.all_to_all(send_rows.reshape(experts, capacity, width), 'ep', split_a...  5.54 us
  transfers between devices with their start and end apart: 6, of which 6 were waited for; matrix products, arithmetic and copies ran while one was open for 16% of the time, Pallas kernels for 0%

commit v1 on v0

v1 whole, which is shorter than its diff:
```python
import functools
import jax
import jax.numpy as jnp
from jax import lax
from jax.experimental import pallas as pl
from jax.experimental.pallas import tpu as pltpu
from jax.sharding import PartitionSpec as P

MESH = pl.DeviceIdType.MESH
CORES = 2
BF = jnp.bfloat16


def place():
    e, t = lax.axis_index("ep"), lax.axis_index("tp")
    return e, t, t // CORES, lax.rem(t, CORES)


def greet(n_ep, n_y, e, t, y, c):
    barrier = pltpu.get_barrier_semaphore()

    def hello(d, carry):
        pl.semaphore_signal(
            barrier, inc=1, device_id=(lax.rem(e + d, n_ep), t), device_id_type=MESH
        )
        return carry

    lax.fori_loop(1, n_ep, hello, 0)
    for j in range(1, n_y):
        other = lax.rem(y + j, n_y) * CORES + c
        pl.semaphore_signal(barrier, inc=1, device_id=(e, other), device_id_type=MESH)
    pl.semaphore_signal(
        barrier, inc=1, device_id=(e, y * CORES + 1 - c), device_id_type=MESH
    )
    pl.semaphore_wait(barrier, n_ep - 1 + n_y - 1 + 1)


def dispatch_kernel(
    n_ep, n_y, send, out, own_sem, ep_s, ep_r, y_s, y_r, c_s, c_r
):
    e, t, y, c = place()
    capp, quarter = send.shape[2], send.shape[3]
    greet(n_ep, n_y, e, t, y, c)
    sibling = (e, y * CORES + 1 - c)

    def zone(source, q):
        return out.at[
            :,
            pl.ds(pl.multiple_of(source * capp, capp), capp),
            pl.ds(pl.multiple_of(q * quarter, quarter), quarter),
        ]

    def over_ep(d):
        to = lax.rem(e + d, n_ep)
        return pltpu.make_async_remote_copy(
            send.at[to], zone(e, t), ep_s.at[d], ep_r.at[d], (to, t), MESH
        )

    def ep_landed(d):
        source = lax.rem(e - d + n_ep, n_ep)
        pltpu.make_async_copy(zone(source, t), zone(source, t), ep_r.at[d]).wait()

    def over_y(d, j):
        source = lax.rem(e - d + n_ep, n_ep)
        to = lax.rem(y + j, n_y) * CORES + c
        return pltpu.make_async_remote_copy(
            zone(source, t), zone(source, t), y_s.at[j, d], y_r.at[j, d], (e, to), MESH
        )

    def y_landed(d, j):
        source = lax.rem(e - d + n_ep, n_ep)
        q = lax.rem(y - j + n_y, n_y) * CORES + c
        pltpu.make_async_copy(zone(source, q), zone(source, q), y_r.at[j, d]).wait()

    def over_core(d, j):
        source = lax.rem(e - d + n_ep, n_ep)
        q = lax.rem(y - j + n_y, n_y) * CORES + c
        return pltpu.make_async_remote_copy(
            zone(source, q), zone(source, q), c_s.at[j, d], c_r.at[j, d], sibling, MESH
        )

    def core_landed(d, j):
        source = lax.rem(e - d + n_ep, n_ep)
        q = lax.rem(y - j + n_y, n_y) * CORES + 1 - c
        pltpu.make_async_copy(zone(source, q), zone(source, q), c_r.at[j, d]).wait()

    own = pltpu.make_async_copy(send.at[e], zone(e, t), own_sem)
    own.start()

    def start_ep(d, carry):
        over_ep(d).start()
        return carry

    lax.fori_loop(1, n_ep, start_ep, 0)
    own.wait()
    for j in range(1, n_y):
        over_y(0, j).start()
    over_core(0, 0).start()

    def step(d, carry):
        ep_landed(d)
        for j in range(1, n_y):
            over_y(d, j).start()
        over_core(d, 0).start()
        for j in range(1, n_y):
            y_landed(d - 1, j)
            over_core(d - 1, j).start()
        return carry

    lax.fori_loop(1, n_ep, step, 0)
    for j in range(1, n_y):
        y_landed(n_ep - 1, j)
        over_core(n_ep - 1, j).start()

    def finish(d, carry):
        for j in range(n_y):
            core_landed(d, j)
            over_core(d, j).wait_send()
        for j in range(1, n_y):
            over_y(d, j).wait_send()
        return carry

    lax.fori_loop(0, n_ep, finish, 0)

    def finish_ep(d, carry):
        over_ep(d).wait_send()
        return carry

    lax.fori_loop(1, n_ep, finish_ep, 0)


def dispatch(send, n_ep, n_tp):
    n_y = n_tp // CORES
    capp, quarter = send.shape[2], send.shape[3]
    return pl.pallas_call(
        functools.partial(dispatch_kernel, n_ep, n_y),
        out_shape=jax.ShapeDtypeStruct((2, n_ep * capp, quarter * n_tp), BF),
        in_specs=[pl.BlockSpec(memory_space=pltpu.VMEM)],
        out_specs=pl.BlockSpec(memory_space=pltpu.VMEM),
        scratch_shapes=[
            pltpu.SemaphoreType.DMA,
            pltpu.SemaphoreType.DMA((n_ep,)),
            pltpu.SemaphoreType.DMA((n_ep,)),
            pltpu.SemaphoreType.DMA((n_y, n_ep)),
            pltpu.SemaphoreType.DMA((n_y, n_ep)),
            pltpu.SemaphoreType.DMA((n_y, n_ep)),
            pltpu.SemaphoreType.DMA((n_y, n_ep)),
        ],
        compiler_params=pltpu.CompilerParams(collective_id=0, has_side_effects=True),
        name="dispatch",
    )(send)


def combine_kernel(
    n_ep,
    n_y,
    cap,
    part,
    pick,
    tokens_out,
    slots_out,
    from_core,
    pair,
    from_y,
    total,
    home,
    a_s,
    a_r,
    b_s,
    b_r,
    h_s,
    h_r,
    g_s,
    g_r,
    k_s,
    k_r,
):
    e, t, y, c = place()
    capp, quarter = home.shape[1], home.shape[2]
    greet(n_ep, n_y, e, t, y, c)
    sibling = (e, y * CORES + 1 - c)

    def zone(b, q):
        return part.at[
            pl.ds(pl.multiple_of(b * capp, capp), capp),
            pl.ds(pl.multiple_of(q * quarter, quarter), quarter),
        ]

    def block(d):
        return lax.rem(e + d, n_ep)

    def to_core(d, j):
        q = lax.rem(y + j, n_y) * CORES + 1 - c
        return pltpu.make_async_remote_copy(
            zone(block(d), q), from_core.at[j, d], a_s.at[j, d], a_r.at[j, d], sibling, MESH
        )

    def to_y(d, j):
        q = lax.rem(y + j, n_y) * CORES + c
        return pltpu.make_async_remote_copy(
            pair.at[j, d], from_y.at[j, d], b_s.at[j, d], b_r.at[j, d], (e, q), MESH
        )

    def to_home(d):
        return pltpu.make_async_remote_copy(
            total.at[d], home.at[e], h_s.at[d], h_r.at[d], (block(d), t), MESH
        )

    def mine(d, j):
        q = lax.rem(y + j, n_y) * CORES + c
        return zone(block(d), q)[...].astype(jnp.float32) + from_core[j, d].astype(
            jnp.float32
        )

    def first(d, carry):
        for j in range(n_y):
            to_core(d, (j + 1) % n_y).start()
        return carry

    lax.fori_loop(1, n_ep, first, 0)
    first(0, 0)

    def second(d, carry):
        for j in range(1, n_y):
            to_core(d, j).wait()
            pair[j, d] = mine(d, j).astype(BF)
            to_y(d, j).start()
        return carry

    lax.fori_loop(1, n_ep, second, 0)
    second(0, 0)

    def added(d):
        to_core(d, 0).wait()
        value = mine(d, 0)
        for j in range(1, n_y):
            to_y(d, j).wait()
            value = value + from_y[j, d].astype(jnp.float32)
        return value.astype(BF)

    def third(d, carry):
        total[d] = added(d)
        to_home(d).start()
        return carry

    lax.fori_loop(1, n_ep, third, 0)
    home[e] = added(0)

    def landed(d, carry):
        source = lax.rem(e - d + n_ep, n_ep)
        pltpu.make_async_copy(home.at[source], home.at[source], h_r.at[d]).wait()
        return carry

    lax.fori_loop(1, n_ep, landed, 0)

    def columns(q):
        return tokens_out.at[:, pl.ds(pl.multiple_of(q * quarter, quarter), quarter)]

    columns(t)[...] = jnp.dot(
        pick[...],
        home[...].reshape(n_ep * capp, quarter),
        preferred_element_type=jnp.float32,
    ).astype(BF)

    def gather_y(j):
        q = lax.rem(y + j, n_y) * CORES + c
        return pltpu.make_async_remote_copy(
            columns(t), columns(t), g_s.at[j], g_r.at[j], (e, q), MESH
        )

    def gather_core(j):
        q = lax.rem(y - j + n_y, n_y) * CORES + c
        return pltpu.make_async_remote_copy(
            columns(q), columns(q), k_s.at[j], k_r.at[j], sibling, MESH
        )

    for j in range(1, n_y):
        gather_y(j).start()
    gather_core(0).start()
    slots_out[...] = home[:, cap, :]
    for j in range(1, n_y):
        q = lax.rem(y - j + n_y, n_y) * CORES + c
        pltpu.make_async_copy(columns(q), columns(q), g_r.at[j]).wait()
        gather_core(j).start()
    for j in range(n_y):
        q = lax.rem(y - j + n_y, n_y) * CORES + 1 - c
        pltpu.make_async_copy(columns(q), columns(q), k_r.at[j]).wait()
        gather_core(j).wait_send()
    for j in range(1, n_y):
        gather_y(j).wait_send()

    def finish(d, carry):
        to_home(d).wait_send()
        return carry

    lax.fori_loop(1, n_ep, finish, 0)


def combine(part, pick, cap, n_ep, n_tp):
    n_y = n_tp // CORES
    capp = part.shape[0] // n_ep
    width = part.shape[1]
    quarter = width // n_tp
    dma = pltpu.SemaphoreType.DMA
    vmem = pl.BlockSpec(memory_space=pltpu.VMEM)
    return pl.pallas_call(
        functools.partial(combine_kernel, n_ep, n_y, cap),
        out_shape=(
            jax.ShapeDtypeStruct((pick.shape[0], width), BF),
            jax.ShapeDtypeStruct((n_ep, quarter), BF),
        ),
        in_specs=[vmem, vmem],
        out_specs=(vmem, vmem),
        scratch_shapes=[
            pltpu.VMEM((n_y, n_ep, capp, quarter), BF),
            pltpu.VMEM((n_y, n_ep, capp, quarter), BF),
            pltpu.VMEM((n_y, n_ep, capp, quarter), BF),
            pltpu.VMEM((n_ep, capp, quarter), BF),
            pltpu.VMEM((n_ep, capp, quarter), BF),
            dma((n_y, n_ep)),
            dma((n_y, n_ep)),
            dma((n_y, n_ep)),
            dma((n_y, n_ep)),
            dma((n_ep,)),
            dma((n_ep,)),
            dma((n_y,)),
            dma((n_y,)),
            dma((n_y,)),
            dma((n_y,)),
        ],
        compiler_params=pltpu.CompilerParams(collective_id=1, has_side_effects=True),
        name="combine",
    )(part, pick)


def on_device(tokens, cotangent, routing, route_weights, w_gate, w_up, w_down):
    n_ep, n_tp = lax.axis_size("ep"), lax.axis_size("tp")
    t = lax.axis_index("tp")
    local_tokens, top_count = routing.shape
    width = tokens.shape[1]
    quarter = width // n_tp
    cap = max(2, (5 * local_tokens * top_count + 4 * n_ep - 1) // (4 * n_ep))
    capp = (cap + 1 + 15) // 16 * 16
    slots = n_ep * capp
    experts = jnp.arange(n_ep, dtype=jnp.int32)
    named = [routing[:, k, None] == experts[None, :] for k in range(top_count)]
    any_named = functools.reduce(jnp.logical_or, named)
    order = jnp.arange(local_tokens, dtype=jnp.int32)
    earlier = (order[:, None] > order[None, :]).astype(BF)
    before = jnp.dot(earlier, any_named.astype(BF), preferred_element_type=jnp.float32)
    targets = [
        jnp.sum(
            jnp.where(n, before.astype(jnp.int32) + experts[None, :] * capp, 0), axis=1
        )
        for n in named
    ]
    slot_ids = jnp.arange(slots, dtype=jnp.int32)
    chosen = [target[:, None] == slot_ids[None, :] for target in targets]
    pick = functools.reduce(jnp.logical_or, chosen).astype(BF)
    slot_weight = sum(
        jnp.sum(jnp.where(ch, route_weights[:, k, None], 0.0), axis=0)
        for k, ch in enumerate(chosen)
    ).astype(BF)
    spare = (jnp.arange(capp) == cap)[None, :, None]

    mine = jnp.concatenate(
        [
            lax.dynamic_slice_in_dim(tokens, t * quarter, quarter, 1)[None],
            lax.dynamic_slice_in_dim(cotangent, t * quarter, quarter, 1)[None],
        ],
        0,
    )
    sent = jnp.einsum("ts,atd->asd", pick, mine, preferred_element_type=jnp.float32).astype(BF)
    sent = sent.reshape(2, n_ep, capp, quarter)
    weight_row = jnp.pad(slot_weight.reshape(n_ep, 1, capp), ((0, 0), (0, 0), (0, quarter - capp)))
    send = jnp.stack([jnp.where(spare, weight_row, sent[0]), sent[1]], axis=1)

    both = dispatch(send, n_ep, n_tp)
    rows, back = both[0], both[1]
    weight = rows.reshape(n_ep, capp, width)[:, cap, :capp].reshape(slots, 1).astype(jnp.float32)
    wgate, wup, wdown = w_gate[0], w_up[0], w_down[0]
    pre_gate = jnp.dot(rows, wgate, preferred_element_type=jnp.float32)
    pre_up = jnp.dot(rows, wup, preferred_element_type=jnp.float32)
    along = jnp.einsum("rd,fd->rf", back, wdown, preferred_element_type=jnp.float32)
    gate_sig = jax.nn.sigmoid(pre_gate)
    gate_act = pre_gate * gate_sig
    hidden = gate_act * pre_up
    hidden_grad = weight * along
    gate_grad = (hidden_grad * pre_up * gate_sig * (1.0 + pre_gate * (1.0 - gate_sig))).astype(BF)
    up_grad = (hidden_grad * gate_act).astype(BF)
    scaled = (weight * hidden).astype(BF)
    row_part = jnp.einsum(
        "rf,df->rd", gate_grad, wgate, preferred_element_type=jnp.float32
    ) + jnp.einsum("rf,df->rd", up_grad, wup, preferred_element_type=jnp.float32)
    slot_part = jnp.sum(hidden * along, axis=1).astype(BF)
    slot_row = jnp.pad(slot_part.reshape(n_ep, 1, capp), ((0, 0), (0, 0), (0, quarter - capp)))
    part = jnp.where(
        spare, jnp.tile(slot_row, (1, 1, n_tp)), row_part.astype(BF).reshape(n_ep, capp, width)
    ).reshape(slots, width)
    grad_tokens, slot_home = combine(part, pick, cap, n_ep, n_tp)
    slot_grad = slot_home[:, :capp].reshape(1, slots).astype(jnp.float32)
    grad_weights = jnp.stack(
        [jnp.sum(jnp.where(ch, slot_grad, 0.0), axis=1) for ch in chosen], axis=1
    ).astype(BF)
    grad_gate = jnp.einsum("rd,rf->df", rows, gate_grad, preferred_element_type=jnp.float32).astype(BF)
    grad_up = jnp.einsum("rd,rf->df", rows, up_grad, preferred_element_type=jnp.float32).astype(BF)
    grad_down = jnp.einsum("rf,rd->fd", scaled, back, preferred_element_type=jnp.float32).astype(BF)
    return (grad_tokens, grad_weights, grad_gate[None], grad_up[None], grad_down[None])


def solution(mesh):
    return jax.shard_map(
        on_device,
        mesh=mesh,
        in_specs=(
            P("ep", None),
            P("ep", None),
            P("ep", None),
            P("ep", None),
            P("ep", None, "tp"),
            P("ep", None, "tp"),
            P("ep", "tp", None),
        ),
        out_specs=(
            P("ep", None),
            P("ep", None),
            P("ep", None, "tp"),
            P("ep", None, "tp"),
            P("ep", "tp", None),
        ),
        check_vma=False,
    )
```

time: 212 us -> 118 us (0.56)
  waiting for transfers between devices: 102 us -> 0 us
  Pallas kernels: 0 us -> 77.2 us
  starting transfers between devices: 27.6 us -> 0 us
  between operations: 14.2 us -> 0.77 us
  blocking collectives: 13.3 us -> 0 us
  local copies, waits for them, and re-layouts: 22 us -> 8.93 us
  matrix products: 29.2 us -> 25.3 us
    all_to_all x5 -> x0, waiting for transfers between devices: 89.9 us -> none  [the longest x1 43.1 us: on_device(): lax.all_to_all(send_rows.reshape(experts, capacity, width), 'ep', split_a...]
    pallas_call x0 -> x2, Pallas kernels: none -> 77.2 us  [the longest x1 42.1 us: dispatch(): pl.pallas_call(functools.partial(dispatch_kernel, n_ep, n_y), out_shape=j...]
    all_to_all x5 -> x0, starting transfers between devices: 27.5 us -> none  [the longest x1 7.28 us: on_device(): lax.all_to_all(slot_weight.reshape(experts, capacity), 'ep', split_axis=0...]
    reduce_scatter x1 -> x0, waiting for transfers between devices: 12.6 us -> none  [on_device(): lax.psum_scatter(row_part.reshape(experts, capacity, width).astype(jnp.bf...]
    reshape x7 -> x0, local copies, waits for them, and re-layouts: 11.1 us -> none  [the longest x1 2.72 us: on_device(): rows = rows_in.reshape(slot_total, width)]
    all_gather x1 -> x0, blocking collectives: 7.65 us -> none  [on_device(): grad_tokens = lax.all_gather(feature_part, 'tp', axis=1, tiled=True)]
    psum x1 -> x0, blocking collectives: 5.65 us -> none  [on_device(): slot_sum = lax.psum(slot_part.astype(jnp.bfloat16), 'tp')]
    dot_general x3 -> x2, matrix products: 5.36 us -> 0.76 us  [the longest x1 0.58 us: on_device(): jnp.einsum('ts,atd->asd', pick, mine, preferred_element_type=jnp.float32)]
  transfers between devices with their start and end apart: 6 -> 0, of which waited for: 6 -> 0; matrix products, arithmetic and copies ran while one was open for 16% -> 0% of each run, Pallas kernels for 0% -> 0%
where the time goes in v1:
time: 118 us; the launch traced here: 116 us
  Pallas kernels  77.2 us (65%)
  matrix products  25.3 us (21%)
  local copies, waits for them, and re-layouts  8.93 us (8%)
  other arithmetic  3.69 us (3%)
    pallas_call x1, Pallas kernels, dispatch(): pl.pallas_call(functools.partial(dispatch_kernel, n_ep, n_y), out_shape=j...  42.1 us
    pallas_call x1, Pallas kernels, combine(): pl.pallas_call(functools.partial(combine_kernel, n_ep, n_y, cap), out_sha...  35.1 us
    dot_general x1, matrix products, on_device(): jnp.einsum('rf,df->rd', up_grad, wup, preferred_element_type=jnp.float32)  6.63 us
    dot_general x1, matrix products, on_device(): jnp.einsum('rd,fd->rf', back, wdown, preferred_element_type=jnp.float32)  3.65 us
    dot_general x1, matrix products, on_device(): jnp.einsum('rf,df->rd', gate_grad, wgate, preferred_element_type=jnp.floa...  3.23 us
    dot_general x1, matrix products, on_device(): jnp.einsum('rd,rf->df', rows, up_grad, preferred_element_type=jnp.float32)  2.63 us
    dot_general x1, matrix products, on_device(): jnp.einsum('rd,rf->df', rows, gate_grad, preferred_element_type=jnp.float32)  2.63 us
    dot_general x1, matrix products, on_device(): jnp.einsum('rf,rd->fd', scaled, back, preferred_element_type=jnp.float32)  2.62 us

profile of v1, /device:TPU:0, one launch (start us, length us, event | category | flops | bytes accessed | tf_op | source)
XLA Modules:
  0.0 115.8 jit_solution(10746896124990334943)
XLA Ops:
  0.6 0.9 fusion.48
  1.5 0.2 select_reduce_fusion.5
  1.7 0.8 fusion.47
  2.5 0.2 select_reduce_fusion.2
  2.7 0.1 convert_element_type.90
  2.7 1.0 dynamic-slice_bitcast_fusion
  3.8 0.6 fusion.21
  4.4 0.1 fusion.46
  4.5 0.1 broadcast_select_fusion
  4.6 1.1 pad_maximum_fusion.send
  5.7 42.1 %dispatch.1 = bf16[2,512,2048]{2,1,0:T(8,128)(2,1)} custom-call(bf16[8,2,64,512]{3,2,1,0:T(8,128)(2,1)} %pad_maximum_fusion.send), custom_call_target="tpu_custom_call" | custom-call | tf_op jit(solution)/shard_map/dispatch/pallas_call | solution.py:135
  47.8 1.6 %slice-done = bf16[1,512,2048]{2,1,0:T(8,128)(2,1)S(1)} async-done(((bf16[2,512,2048]{2,1,0:T(8,128)(2,1)}), bf16[1,512,2048]{2,1,0:T(8,128)(2,1)S(1)}, s32[]{:S(2)}) %slice-start) | async-done | bytes 2097176 | tf_op jit(solution)/shard_map/slice | solution.py:379
  49.4 0.1 reshape.100
  49.4 3.6 %fusion.4 = f32[512,512]{0,1:T(8,128)S(1)} fusion(bf16[1,512,2048]{2,1,0:T(8,128)(2,1)} %param.13, bf16[2,512,2048]{2,1,0:T(8,128)(2,1)} %dispatch.1), kind=kOutput, calls=%fused_computation.8 | convolution fusion | flops 1073741824 | bytes 5242880 | tf_op jit(solution)/shard_map/rd,fd->rf/dot_general | solution.py:384
  53.1 0.5 copy-done.2
  53.6 1.3 %fusion.9 = f32[512,512]{0,1:T(8,128)S(1)} fusion(bf16[1,2048,512]{2,1,0:T(8,128)(2,1)S(1)} %copy-done.2, bf16[2,512,2048]{2,1,0:T(8,128)(2,1)S(1)} %copy-done.1), kind=kOutput, calls=%fused_computation.13 | convolution fusion | flops 1073741824 | bytes 5242880 | tf_op jit(solution)/shard_map/dot_general | solution.py:383
  54.9 1.8 %multiply_convert_fusion.2 = (bf16[512,512]{0,1:T(8,128)(2,1)S(1)}, bf16[512]{0:T(512)(128)(2,1)S(1)}, bf16[512,512]{0,1:T(8,128)(2,1)S(1)}, f32[512,512]{0,1:T(8,128)S(1)}) fusion(f32[512,512]{0,1:T(8,128)S(1)} %fusion.9, f32[512,512]{0,1:T(8,128)S(1)} %fusion.4, f32[512]{0:T(512)S(1)} %reshape.100, bf16[1,2048,512]{2,1,0:T(8,128)(2,1)S(1)} %copy-done, ...), kind=kOutput, calls=%fused_computation.32 | convolution fusion | flops 1078197760 | bytes 8391680 | tf_op jit(solution)/shard_map/dot_general | solution.py:382
  56.7 2.6 %fusion.2 = bf16[1,512,2048]{2,1,0:T(8,128)(2,1)} fusion(bf16[2,512,2048]{2,1,0:T(8,128)(2,1)S(1)} %copy-done.1, f32[512]{0:T(512)S(1)} %reshape.100, f32[512,512]{0,1:T(8,128)S(1)} %fusion.9, f32[512,512]{0,1:T(8,128)S(1)} %get-tuple-element.22), kind=kOutput, calls=%fused_computation.6 | convolution fusion | flops 1076625408 | bytes 6293504 | tf_op jit(solution)/shard_map/rf,rd->fd/dot_general | solution.py:407
  59.3 2.6 %fusion = bf16[1,2048,512]{2,1,0:T(8,128)(2,1)} fusion(bf16[512,512]{0,1:T(8,128)(2,1)S(1)} %get-tuple-element.13, bf16[2,512,2048]{2,1,0:T(8,128)(2,1)S(1)} %copy-done.1), kind=kOutput, calls=%fused_computation.4 | convolution fusion | flops 1074790400 | bytes 4718592 | tf_op jit(solution)/shard_map/rd,rf->df/dot_general | solution.py:405
  61.9 2.6 %fusion.1 = bf16[1,2048,512]{2,1,0:T(8,128)(2,1)} fusion(bf16[512,512]{0,1:T(8,128)(2,1)S(1)} %get-tuple-element.15, bf16[2,512,2048]{2,1,0:T(8,128)(2,1)S(1)} %copy-done.1), kind=kOutput, calls=%fused_computation.5 | convolution fusion | flops 1074790400 | bytes 4718592 | tf_op jit(solution)/shard_map/rd,rf->df/dot_general | solution.py:406
  64.6 3.2 %fusion.11 = f32[512,2048]{1,0:T(8,128)} fusion(bf16[512,512]{0,1:T(8,128)(2,1)S(1)} %get-tuple-element.13, bf16[1,2048,512]{2,1,0:T(8,128)(2,1)S(1)} %copy-done), kind=kOutput, calls=%fused_computation.15 | convolution fusion | flops 1073741824 | bytes 6815744 | tf_op jit(solution)/shard_map/rf,df->rd/dot_general | solution.py:392
  67.8 0.1 convert_element_type.94
  67.9 1.6 %broadcast_in_dim.121 = bf16[8,64,2048]{2,1,0:T(8,128)(2,1)} broadcast(bf16[8,2048]{1,0:T(8,128)(2,1)S(1)} %bitcast.67), dimensions={0,2} | broadcast | bytes 2129920 | tf_op jit(solution)/shard_map/jit(_where)/broadcast_in_dim | solution.py:397
  69.5 0.1 broadcast_in_dim.108
  69.6 6.6 %fusion.3.part = bf16[512,2048]{1,0:T(8,128)(2,1)} fusion(bf16[512,2048]{1,0:T(8,128)(2,1)} %bitcast.64, f32[512,2048]{1,0:T(8,128)} %fusion.11, bf16[512,512]{0,1:T(8,128)(2,1)S(1)} %get-tuple-element.15, bf16[1,2048,512]{2,1,0:T(8,128)(2,1)} %param.12, pred[512]{0:T(512)(128)(4,1)S(1)} %broadcast_in_dim.108), kind=kOutput, calls=%fused_computation.7 | convolution fusion | flops 1076887552 | bytes 11010560 | tf_op jit(solution)/shard_map/rf,df->rd/dot_general | solution.py:394
  76.2 0.8 fusion.31.pick
  77.0 35.1 %combine.1 = (bf16[192,2048]{1,0:T(8,128)(2,1)}, bf16[8,512]{1,0:T(8,128)(2,1)}) custom-call(bf16[512,2048]{1,0:T(8,128)(2,1)} %fusion.3.part, bf16[192,512]{1,0:T(8,128)(2,1)} %fusion.31.pick), custom_call_target="tpu_custom_call" | custom-call | tf_op jit(solution)/shard_map/combine/pallas_call | solution.py:306
  112.1 0.7 slice_convert_fusion.1
  112.8 0.1 reshape.101
  112.9 0.3 select_reduce_fusion.1
  113.2 0.6 pad_maximum_fusion.1
  113.7 2.1 %copy.13 = bf16[192,2048]{1,0:T(8,128)(2,1)} copy(bf16[192,2048]{1,0:T(8,128)(2,1)} %get-tuple-element.32) | data formatting | bytes 1572864
  (16 shorter events, 0.1 us)
Async XLA Ops:
  0.6 54.2 %copy-start = (bf16[1,2048,512]{2,1,0:T(8,128)(2,1)S(1)}, bf16[1,2048,512]{2,1,0:T(8,128)(2,1)}, u32[]{:S(2)}) copy-start(bf16[1,2048,512]{2,1,0:T(8,128)(2,1)} %param.11) | copy-start | bytes 6291460
  47.7 1.6 %slice-start = ((bf16[2,512,2048]{2,1,0:T(8,128)(2,1)}), bf16[1,512,2048]{2,1,0:T(8,128)(2,1)S(1)}, s32[]{:S(2)}) async-start(bf16[2,512,2048]{2,1,0:T(8,128)(2,1)} %dispatch.1), calls=%async_computation | async-start | bytes 4194304 | tf_op jit(solution)/shard_map/slice | solution.py:379
  49.4 3.7 %copy-start.1 = (bf16[2,512,2048]{2,1,0:T(8,128)(2,1)S(1)}, bf16[2,512,2048]{2,1,0:T(8,128)(2,1)}, u32[]{:S(2)}) copy-start(bf16[2,512,2048]{2,1,0:T(8,128)(2,1)} %dispatch.1) | copy-start | bytes 12582916
  49.4 4.1 %copy-start.2 = (bf16[1,2048,512]{2,1,0:T(8,128)(2,1)S(1)}, bf16[1,2048,512]{2,1,0:T(8,128)(2,1)}, u32[]{:S(2)}) copy-start(bf16[1,2048,512]{2,1,0:T(8,128)(2,1)} %param.12) | copy-start | bytes 6291460

commit v2 on v1

--- a/solution.py
+++ b/solution.py
@@ -16,6 +16,17 @@
     return e, t, t // CORES, lax.rem(t, CORES)
 
 
+def partner(e, d, n_ep, back):
+    if n_ep & (n_ep - 1):
+        return lax.rem(e + n_ep - d, n_ep) if back else lax.rem(e + d, n_ep)
+    found, bit = 0, 1
+    while bit < n_ep:
+        mine, other = lax.rem(e // bit, 2), lax.rem(d // bit, 2)
+        found = found + bit * lax.rem(mine + other, 2)
+        bit *= 2
+    return found
+
+
 def greet(n_ep, n_y, e, t, y, c):
     barrier = pltpu.get_barrier_semaphore()
 
@@ -51,36 +62,36 @@
         ]
 
     def over_ep(d):
-        to = lax.rem(e + d, n_ep)
+        to = partner(e, d, n_ep, False)
         return pltpu.make_async_remote_copy(
             send.at[to], zone(e, t), ep_s.at[d], ep_r.at[d], (to, t), MESH
         )
 
     def ep_landed(d):
-        source = lax.rem(e - d + n_ep, n_ep)
+        source = partner(e, d, n_ep, True)
         pltpu.make_async_copy(zone(source, t), zone(source, t), ep_r.at[d]).wait()
 
     def over_y(d, j):
-        source = lax.rem(e - d + n_ep, n_ep)
+        source = partner(e, d, n_ep, True)
         to = lax.rem(y + j, n_y) * CORES + c
         return pltpu.make_async_remote_copy(
             zone(source, t), zone(source, t), y_s.at[j, d], y_r.at[j, d], (e, to), MESH
         )
 
     def y_landed(d, j):
-        source = lax.rem(e - d + n_ep, n_ep)
+        source = partner(e, d, n_ep, True)
         q = lax.rem(y - j + n_y, n_y) * CORES + c
         pltpu.make_async_copy(zone(source, q), zone(source, q), y_r.at[j, d]).wait()
 
     def over_core(d, j):
-        source = lax.rem(e - d + n_ep, n_ep)
+        source = partner(e, d, n_ep, True)
         q = lax.rem(y - j + n_y, n_y) * CORES + c
         return pltpu.make_async_remote_copy(
             zone(source, q), zone(source, q), c_s.at[j, d], c_r.at[j, d], sibling, MESH
         )
 
     def core_landed(d, j):
-        source = lax.rem(e - d + n_ep, n_ep)
+        source = partner(e, d, n_ep, True)
         q = lax.rem(y - j + n_y, n_y) * CORES + 1 - c
         pltpu.make_async_copy(zone(source, q), zone(source, q), c_r.at[j, d]).wait()
 
@@ -155,10 +166,15 @@
     n_ep,
     n_y,
     cap,
-    part,
+    gate_grad,
+    up_grad,
+    w_gate,
+    w_up,
+    slot_row,
     pick,
     tokens_out,
     slots_out,
+    part,
     from_core,
     pair,
     from_y,
@@ -187,7 +203,7 @@
         ]
 
     def block(d):
-        return lax.rem(e + d, n_ep)
+        return partner(e, d, n_ep, False)
 
     def to_core(d, j):
         q = lax.rem(y + j, n_y) * CORES + 1 - c
@@ -212,23 +228,41 @@
             jnp.float32
         )
 
-    def first(d, carry):
-        for j in range(n_y):
-            to_core(d, (j + 1) % n_y).start()
-        return carry
-
-    lax.fori_loop(1, n_ep, first, 0)
-    first(0, 0)
-
-    def second(d, carry):
+    def multiply(q):
+        held = pl.ds(pl.multiple_of(q * quarter, quarter), quarter)
+        across = (((1,), (1,)), ((), ()))
+        value = lax.dot_general(
+            gate_grad[...], w_gate[held, :], across, preferred_element_type=jnp.float32
+        ) + lax.dot_general(
+            up_grad[...], w_up[held, :], across, preferred_element_type=jnp.float32
+        )
+        value = value.reshape(n_ep, capp, quarter)
+        spare = lax.broadcasted_iota(jnp.int32, value.shape, 1) == cap
+        value = jnp.where(spare, slot_row[...], value)
+        part[:, held] = value.reshape(n_ep * capp, quarter).astype(BF)
+
+    for i in range(n_y):
+        j = (i + 1) % n_y
+        multiply(lax.rem(y + j, n_y) * CORES + 1 - c)
+
+        def first(i, carry):
+            to_core(n_ep - 1 - i, j).start()
+            return carry
+
+        lax.fori_loop(0, n_ep, first, 0)
+    for i in range(n_y - 1):
+        multiply(lax.rem(y + i + 1, n_y) * CORES + c)
+
+    def second(i, carry):
+        d = n_ep - 1 - i
         for j in range(1, n_y):
             to_core(d, j).wait()
             pair[j, d] = mine(d, j).astype(BF)
             to_y(d, j).start()
         return carry
 
-    lax.fori_loop(1, n_ep, second, 0)
-    second(0, 0)
+    lax.fori_loop(0, n_ep, second, 0)
+    multiply(y * CORES + c)
 
     def added(d):
         to_core(d, 0).wait()
@@ -238,7 +272,8 @@
             value = value + from_y[j, d].astype(jnp.float32)
         return value.astype(BF)
 
-    def third(d, carry):
+    def third(i, carry):
+        d = n_ep - i
         total[d] = added(d)
         to_home(d).start()
         return carry
@@ -247,7 +282,7 @@
     home[e] = added(0)
 
     def landed(d, carry):
-        source = lax.rem(e - d + n_ep, n_ep)
+        source = partner(e, d, n_ep, True)
         pltpu.make_async_copy(home.at[source], home.at[source], h_r.at[d]).wait()
         return carry
 
@@ -296,10 +331,10 @@
     lax.fori_loop(1, n_ep, finish, 0)
 
 
-def combine(part, pick, cap, n_ep, n_tp):
+def combine(gate_grad, up_grad, w_gate, w_up, slot_row, pick, cap, n_ep, n_tp):
     n_y = n_tp // CORES
-    capp = part.shape[0] // n_ep
-    width = part.shape[1]
+    capp = gate_grad.shape[0] // n_ep
+    width = w_gate.shape[0]
     quarter = width // n_tp
     dma = pltpu.SemaphoreType.DMA
     vmem = pl.BlockSpec(memory_space=pltpu.VMEM)
@@ -309,9 +344,10 @@
             jax.ShapeDtypeStruct((pick.shape[0], width), BF),
             jax.ShapeDtypeStruct((n_ep, quarter), BF),
         ),
-        in_specs=[vmem, vmem],
+        in_specs=[vmem] * 6,
         out_specs=(vmem, vmem),
         scratch_shapes=[
+            pltpu.VMEM((n_ep * capp, width), BF),
             pltpu.VMEM((n_y, n_ep, capp, quarter), BF),
             pltpu.VMEM((n_y, n_ep, capp, quarter), BF),
             pltpu.VMEM((n_y, n_ep, capp, quarter), BF),
@@ -330,7 +366,7 @@
         ],
         compiler_params=pltpu.CompilerParams(collective_id=1, has_side_effects=True),
         name="combine",
-    )(part, pick)
+    )(gate_grad, up_grad, w_gate, w_up, slot_row, pick)
 
 
 def on_device(tokens, cotangent, routing, route_weights, w_gate, w_up, w_down):
@@ -389,15 +425,11 @@
     gate_grad = (hidden_grad * pre_up * gate_sig * (1.0 + pre_gate * (1.0 - gate_sig))).astype(BF)
     up_grad = (hidden_grad * gate_act).astype(BF)
     scaled = (weight * hidden).astype(BF)
-    row_part = jnp.einsum(
-        "rf,df->rd", gate_grad, wgate, preferred_element_type=jnp.float32
-    ) + jnp.einsum("rf,df->rd", up_grad, wup, preferred_element_type=jnp.float32)
-    slot_part = jnp.sum(hidden * along, axis=1).astype(BF)
+    slot_part = jnp.sum(hidden * along, axis=1)
     slot_row = jnp.pad(slot_part.reshape(n_ep, 1, capp), ((0, 0), (0, 0), (0, quarter - capp)))
-    part = jnp.where(
-        spare, jnp.tile(slot_row, (1, 1, n_tp)), row_part.astype(BF).reshape(n_ep, capp, width)
-    ).reshape(slots, width)
-    grad_tokens, slot_home = combine(part, pick, cap, n_ep, n_tp)
+    grad_tokens, slot_home = combine(
+        gate_grad, up_grad, wgate, wup, slot_row, pick, cap, n_ep, n_tp
+    )
     slot_grad = slot_home[:, :capp].reshape(1, slots).astype(jnp.float32)
     grad_weights = jnp.stack(
         [jnp.sum(jnp.where(ch, slot_grad, 0.0), axis=1) for ch in chosen], axis=1

time: 118 us -> 100 us (0.85); the launches traced: 116 us -> 100 us
  matrix products: 25.3 us -> 15.6 us
  Pallas kernels: 77.2 us -> 72.1 us
    dot_general x2 -> x0, matrix products: 9.86 us -> none  [the longest x1 6.63 us: on_device(): jnp.einsum('rf,df->rd', up_grad, wup, preferred_element_type=jnp.float32)]
    pallas_call x1, Pallas kernels: 42.1 us -> 39.3 us  [dispatch(): pl.pallas_call(functools.partial(dispatch_kernel, n_ep, n_y), out_shape=j...]
    pallas_call x1, Pallas kernels: 35.1 us -> 32.8 us  [combine(): pl.pallas_call(functools.partial(combine_kernel, n_ep, n_y, cap), out_sha...]
    dot_general x1, matrix products: 1.81 us -> 3.61 us  [on_device(): pre_gate = jnp.dot(rows, wgate, preferred_element_type=jnp.float32)]
    dot_general x1, matrix products: 3.65 us -> 1.92 us  [on_device(): jnp.einsum('rd,fd->rf', back, wdown, preferred_element_type=jnp.float32)]
    broadcast_in_dim x3 -> x0, local copies, waits for them, and re-layouts: 1.69 us -> none  [on_device(): jnp.where(spare, jnp.tile(slot_row, (1, 1, n_tp)), row_part.astype(BF).re...]
    unnamed x7 -> x11, local copies, waits for them, and re-layouts: 2.56 us -> 2.61 us
where the time goes in v2:
time: 100 us
  Pallas kernels  72.1 us (72%)
  matrix products  15.6 us (16%)
  local copies, waits for them, and re-layouts  7.87 us (8%)
  other arithmetic  3.67 us (4%)
    pallas_call x1, Pallas kernels, dispatch(): pl.pallas_call(functools.partial(dispatch_kernel, n_ep, n_y), out_shape=j...  39.3 us
    pallas_call x1, Pallas kernels, combine(): pl.pallas_call(functools.partial(combine_kernel, n_ep, n_y, cap), out_sha...  32.8 us
    dot_general x1, matrix products, on_device(): pre_gate = jnp.dot(rows, wgate, preferred_element_type=jnp.float32)  3.61 us
    dot_general x1, matrix products, on_device(): jnp.einsum('rf,rd->fd', scaled, back, preferred_element_type=jnp.float32)  2.81 us
    dot_general x1, matrix products, on_device(): jnp.einsum('rd,rf->df', rows, gate_grad, preferred_element_type=jnp.float32)  2.64 us
    dot_general x1, matrix products, on_device(): jnp.einsum('rd,rf->df', rows, up_grad, preferred_element_type=jnp.float32)  2.64 us
    unnamed x11, local copies, waits for them, and re-layouts  2.61 us

profile of v2, /device:TPU:0, one launch (start us, length us, event | category | flops | bytes accessed | tf_op | source)
XLA Modules:
  0.0 100.0 jit_solution(14206147653196731393)
XLA Ops:
  0.6 0.0 copy-start
  0.6 0.9 fusion.44
  1.5 0.2 select_reduce_fusion.5
  1.7 0.8 fusion.43
  2.5 0.2 select_reduce_fusion.2
  2.7 0.1 convert_element_type.75
  2.7 1.0 %dynamic-slice_bitcast_fusion = (bf16[1,192,512]{2,1,0:T(8,128)(2,1)S(1)}, bf16[1,192,512]{2,1,0:T(8,128)(2,1)S(1)}) fusion(bf16[192,2048]{1,0:T(8,128)(2,1)} %param.8, s32[]{:T(128)S(6)} %select_n.40, bf16[192,2048]{1,0:T(8,128)(2,1)} %param.7), kind=kLoop, calls=%fused_computation.44 | loop fusion | bytes 786436 | tf_op jit(solution)/shard_map/broadcast_in_dim | solution.py:405
  3.8 0.6 fusion.15
  4.4 0.1 fusion.42
  4.5 0.1 broadcast_select_fusion
  4.6 1.1 %pad_maximum_fusion.send = bf16[8,2,64,512]{3,2,1,0:T(8,128)(2,1)} fusion(bf16[8,1,64,512]{3,2,1,0:T(8,128)(2,1)S(1)} %bitcast.56, bf16[8,1,64,512]{3,2,1,0:T(8,128)(2,1)S(1)} %broadcast_select_fusion), kind=kLoop, calls=%fused_computation.22 | loop fusion | flops 524288 | bytes 2097152 | tf_op jit(solution)/shard_map/stack | solution.py:412
  5.7 39.3 %dispatch.1 = bf16[2,512,2048]{2,1,0:T(8,128)(2,1)} custom-call(bf16[8,2,64,512]{3,2,1,0:T(8,128)(2,1)} %pad_maximum_fusion.send), custom_call_target="tpu_custom_call" | custom-call | tf_op jit(solution)/shard_map/dispatch/pallas_call | solution.py:146
  45.0 0.0 slice-start
  45.0 1.6 %slice-done = bf16[1,512,2048]{2,1,0:T(8,128)(2,1)S(1)} async-done(((bf16[2,512,2048]{2,1,0:T(8,128)(2,1)}), bf16[1,512,2048]{2,1,0:T(8,128)(2,1)S(1)}, s32[]{:S(2)}) %slice-start) | async-done | bytes 2097176 | tf_op jit(solution)/shard_map/slice | solution.py:415
  46.6 0.1 reshape.82
  46.7 3.6 %fusion.5 = f32[512,512]{1,0:T(8,128)S(1)} fusion(bf16[1,2048,512]{2,1,0:T(8,128)(2,1)} %param.11, bf16[2,512,2048]{2,1,0:T(8,128)(2,1)} %dispatch.1), kind=kOutput, calls=%fused_computation.8 | convolution fusion | flops 1073741824 | bytes 5242880 | tf_op jit(solution)/shard_map/dot_general | solution.py:418
  50.3 0.5 copy-done.2
  50.8 1.2 %fusion.7 = f32[512,512]{1,0:T(8,128)S(1)} fusion(bf16[1,2048,512]{2,1,0:T(8,128)(2,1)S(1)} %copy-done.2, bf16[2,512,2048]{2,1,0:T(8,128)(2,1)S(1)} %copy-done.1), kind=kOutput, calls=%fused_computation.10 | convolution fusion | flops 1073741824 | bytes 5242880 | tf_op jit(solution)/shard_map/dot_general | solution.py:419
  52.0 2.8 %fusion.2 = bf16[1,512,2048]{2,1,0:T(8,128)(2,1)} fusion(bf16[2,512,2048]{2,1,0:T(8,128)(2,1)S(1)} %copy-done.1, f32[512]{0:T(512)S(1)} %reshape.82, f32[512,512]{1,0:T(8,128)S(1)} %fusion.7, f32[512,512]{1,0:T(8,128)S(1)} %fusion.5), kind=kOutput, calls=%fused_computation.5 | convolution fusion | flops 1076625408 | bytes 6293504 | tf_op jit(solution)/shard_map/rf,rd->fd/dot_general | solution.py:439
  54.8 1.9 %multiply_reduce_fusion = (f32[512]{0:T(512)S(1)}, bf16[512,512]{1,0:T(8,128)(2,1)S(1)}, bf16[512,512]{1,0:T(8,128)(2,1)S(1)}) fusion(f32[512,512]{1,0:T(8,128)S(1)} %fusion.7, f32[512,512]{1,0:T(8,128)S(1)} %fusion.5, f32[512]{0:T(512)S(1)} %reshape.82, bf16[1,512,2048]{2,1,0:T(8,128)(2,1)S(1)} %copy-done, bf16[2,512,2048]{2,1,0:T(8,128)(2,1)S(1)} %copy-done.1), kind=kOutput, calls=%fused_computation.24 | convolution fusion | flops 1078197760 | bytes 7344128 | tf_op jit(solution)/shard_map/rd,fd->rf/dot_general | solution.py:420
  56.8 0.0 copy-start.3
  56.8 2.6 %fusion.1 = bf16[1,2048,512]{2,1,0:T(8,128)(2,1)} fusion(bf16[512,512]{1,0:T(8,128)(2,1)S(1)} %get-tuple-element.15.up_grad, bf16[2,512,2048]{2,1,0:T(8,128)(2,1)S(1)} %copy-done.1), kind=kOutput, calls=%fused_computation.4 | convolution fusion | flops 1074790400 | bytes 4718592 | tf_op jit(solution)/shard_map/rd,rf->df/dot_general | solution.py:438
  59.4 2.6 %fusion = bf16[1,2048,512]{2,1,0:T(8,128)(2,1)} fusion(bf16[512,512]{1,0:T(8,128)(2,1)S(1)} %get-tuple-element.14.gate_grad, bf16[2,512,2048]{2,1,0:T(8,128)(2,1)S(1)} %copy-done.1), kind=kOutput, calls=%fused_computation.3 | convolution fusion | flops 1074790400 | bytes 4718592 | tf_op jit(solution)/shard_map/rd,rf->df/dot_general | solution.py:437
  62.1 0.1 reshape.81
  62.2 0.6 pad.9.slot_row
  62.8 0.8 fusion.25.pick
  63.6 32.8 %combine.1 = (bf16[192,2048]{1,0:T(8,128)(2,1)}, bf16[8,512]{1,0:T(8,128)(2,1)}) custom-call(bf16[512,512]{1,0:T(8,128)(2,1)} %copy-done.3, bf16[512,512]{1,0:T(8,128)(2,1)} %copy-done.4, bf16[2048,512]{1,0:T(8,128)(2,1)} %bitcast.55, bf16[2048,512]{1,0:T(8,128)(2,1)} %bitcast.54, f32[8,1,512]{2,1,0:T(1,128)} %pad.9.slot_row, bf16[192,512]{1,0:T(8,128)(2,1)} %fusion.25.pick), custom_call_target="tpu_custom_call" | custom-call | tf_op jit(solution)/shard_map/combine/pallas_call | solution.py:341
  96.3 0.7 slice_convert_fusion.1
  97.0 0.1 reshape.83
  97.1 0.3 select_reduce_fusion.1
  97.4 0.6 pad_maximum_fusion.1
  97.9 2.1 %copy.23 = bf16[192,2048]{1,0:T(8,128)(2,1)} copy(bf16[192,2048]{1,0:T(8,128)(2,1)} %get-tuple-element.31) | data formatting | bytes 1572864
  (14 shorter events, 0.1 us)
Async XLA Ops:
  0.6 54.2 %copy-start = (bf16[1,512,2048]{2,1,0:T(8,128)(2,1)S(1)}, bf16[1,512,2048]{2,1,0:T(8,128)(2,1)}, u32[]{:S(2)}) copy-start(bf16[1,512,2048]{2,1,0:T(8,128)(2,1)} %param.13) | copy-start | bytes 6291460
  45.0 1.6 %slice-start = ((bf16[2,512,2048]{2,1,0:T(8,128)(2,1)}), bf16[1,512,2048]{2,1,0:T(8,128)(2,1)S(1)}, s32[]{:S(2)}) async-start(bf16[2,512,2048]{2,1,0:T(8,128)(2,1)} %dispatch.1), calls=%async_computation | async-start | bytes 4194304 | tf_op jit(solution)/shard_map/slice | solution.py:415
  46.7 3.6 %copy-start.1 = (bf16[2,512,2048]{2,1,0:T(8,128)(2,1)S(1)}, bf16[2,512,2048]{2,1,0:T(8,128)(2,1)}, u32[]{:S(2)}) copy-start(bf16[2,512,2048]{2,1,0:T(8,128)(2,1)} %dispatch.1) | copy-start | bytes 12582916
  46.7 4.1 %copy-start.2 = (bf16[1,2048,512]{2,1,0:T(8,128)(2,1)S(1)}, bf16[1,2048,512]{2,1,0:T(8,128)(2,1)}, u32[]{:S(2)}) copy-start(bf16[1,2048,512]{2,1,0:T(8,128)(2,1)} %param.12) | copy-start | bytes 6291460
  56.8 2.7 %copy-start.4 = (bf16[512,512]{1,0:T(8,128)(2,1)}, bf16[512,512]{1,0:T(8,128)(2,1)S(1)}, u32[]{:S(2)}) copy-start(bf16[512,512]{1,0:T(8,128)(2,1)S(1)} %get-tuple-element.15.up_grad) | copy-start | bytes 1572868
  56.8 2.7 %copy-start.3 = (bf16[512,512]{1,0:T(8,128)(2,1)}, bf16[512,512]{1,0:T(8,128)(2,1)S(1)}, u32[]{:S(2)}) copy-start(bf16[512,512]{1,0:T(8,128)(2,1)S(1)} %get-tuple-element.14.gate_grad) | copy-start | bytes 1572868

commit v3 on v2

--- a/solution.py
+++ b/solution.py
@@ -147,7 +147,7 @@
         functools.partial(dispatch_kernel, n_ep, n_y),
         out_shape=jax.ShapeDtypeStruct((2, n_ep * capp, quarter * n_tp), BF),
         in_specs=[pl.BlockSpec(memory_space=pltpu.VMEM)],
-        out_specs=pl.BlockSpec(memory_space=pltpu.VMEM),
+        out_specs=pl.BlockSpec(memory_space=pl.ANY),
         scratch_shapes=[
             pltpu.SemaphoreType.DMA,
             pltpu.SemaphoreType.DMA((n_ep,)),
@@ -157,7 +157,9 @@
             pltpu.SemaphoreType.DMA((n_y, n_ep)),
             pltpu.SemaphoreType.DMA((n_y, n_ep)),
         ],
-        compiler_params=pltpu.CompilerParams(collective_id=0, has_side_effects=True),
+        compiler_params=pltpu.CompilerParams(
+            collective_id=0, has_side_effects=True, vmem_limit_bytes=8 << 20
+        ),
         name="dispatch",
     )(send)
 

time: 100 us -> 96.4 us (0.964)
  Pallas kernels: 72.1 us -> 68.8 us
    pallas_call x1, Pallas kernels: 39.3 us -> 36.3 us  [dispatch(): pl.pallas_call(functools.partial(dispatch_kernel, n_ep, n_y), out_shape=j...]
    unnamed x11 -> x13, local copies, waits for them, and re-layouts: 2.61 us -> 4.28 us
    slice x2 -> x1, local copies, waits for them, and re-layouts: 1.58 us -> 0.24 us  [on_device(): rows, back = (both[0], both[1])]
where the time goes in v3:
time: 96.4 us; the launch traced here: 96.2 us
  Pallas kernels  68.8 us (71%)
  matrix products  15.6 us (16%)
  local copies, waits for them, and re-layouts  8.2 us (9%)
  other arithmetic  2.71 us (3%)
    pallas_call x1, Pallas kernels, dispatch(): pl.pallas_call(functools.partial(dispatch_kernel, n_ep, n_y), out_shape=j...  36.3 us
    pallas_call x1, Pallas kernels, combine(): pl.pallas_call(functools.partial(combine_kernel, n_ep, n_y, cap), out_sha...  32.6 us
    unnamed x13, local copies, waits for them, and re-layouts  4.28 us
    dot_general x1, matrix products, on_device(): pre_gate = jnp.dot(rows, wgate, preferred_element_type=jnp.float32)  3.61 us
    dot_general x1, matrix products, on_device(): jnp.einsum('rf,rd->fd', scaled, back, preferred_element_type=jnp.float32)  2.81 us
    dot_general x1, matrix products, on_device(): jnp.einsum('rd,rf->df', rows, up_grad, preferred_element_type=jnp.float32)  2.64 us
    dot_general x1, matrix products, on_device(): jnp.einsum('rd,rf->df', rows, gate_grad, preferred_element_type=jnp.float32)  2.64 us

profile of v3, /device:TPU:0, one launch (start us, length us, event | category | flops | bytes accessed | tf_op | source)
XLA Modules:
  0.0 96.2 jit_solution(3113088564249964691)
XLA Ops:
  0.6 0.0 copy-start
  0.6 0.9 fusion.44
  1.5 0.2 select_reduce_fusion.5
  1.7 0.8 fusion.43
  2.5 0.2 select_reduce_fusion.2
  2.7 0.1 convert_element_type.75
  2.7 1.0 %dynamic-slice_bitcast_fusion = (bf16[1,192,512]{2,1,0:T(8,128)(2,1)S(1)}, bf16[1,192,512]{2,1,0:T(8,128)(2,1)S(1)}) fusion(bf16[192,2048]{1,0:T(8,128)(2,1)} %param.8, s32[]{:T(128)S(6)} %select_n.40, bf16[192,2048]{1,0:T(8,128)(2,1)} %param.7), kind=kLoop, calls=%fused_computation.44 | loop fusion | bytes 786436 | tf_op jit(solution)/shard_map/broadcast_in_dim | solution.py:407
  3.8 0.6 fusion.15
  4.4 0.1 fusion.42
  4.5 0.1 broadcast_select_fusion
  4.6 0.1 pad_maximum_fusion.send
  4.7 36.3 %dispatch.1 = bf16[2,512,2048]{2,1,0:T(8,128)(2,1)S(1)} custom-call(bf16[8,2,64,512]{3,2,1,0:T(8,128)(2,1)S(1)} %pad_maximum_fusion.send), custom_call_target="tpu_custom_call" | custom-call | tf_op jit(solution)/shard_map/dispatch/pallas_call | solution.py:146
  41.0 0.2 slice.38
  41.2 1.7 %copy-done.1 = bf16[2,512,2048]{2,1,0:T(8,128)(2,1)} copy-done((bf16[2,512,2048]{2,1,0:T(8,128)(2,1)}, bf16[2,512,2048]{2,1,0:T(8,128)(2,1)S(1)}, u32[]{:S(2)}) %copy-start.1) | copy-done | bytes 4194328
  42.9 0.1 reshape.82
  43.0 3.6 %fusion.5 = f32[512,512]{1,0:T(8,128)S(1)} fusion(bf16[1,2048,512]{2,1,0:T(8,128)(2,1)} %param.11, bf16[2,512,2048]{2,1,0:T(8,128)(2,1)} %copy-done.1), kind=kOutput, calls=%fused_computation.8 | convolution fusion | flops 1073741824 | bytes 5242880 | tf_op jit(solution)/shard_map/dot_general | solution.py:420
  46.6 0.5 copy-done.3
  47.1 1.2 %fusion.7 = f32[512,512]{1,0:T(8,128)S(1)} fusion(bf16[1,2048,512]{2,1,0:T(8,128)(2,1)S(1)} %copy-done.3, bf16[2,512,2048]{2,1,0:T(8,128)(2,1)S(1)} %copy-done.2), kind=kOutput, calls=%fused_computation.10 | convolution fusion | flops 1073741824 | bytes 5242880 | tf_op jit(solution)/shard_map/dot_general | solution.py:421
  48.4 2.8 %fusion.2 = bf16[1,512,2048]{2,1,0:T(8,128)(2,1)} fusion(bf16[2,512,2048]{2,1,0:T(8,128)(2,1)S(1)} %copy-done.2, f32[512]{0:T(512)S(1)} %reshape.82, f32[512,512]{1,0:T(8,128)S(1)} %fusion.7, f32[512,512]{1,0:T(8,128)S(1)} %fusion.5), kind=kOutput, calls=%fused_computation.5 | convolution fusion | flops 1076625408 | bytes 6293504 | tf_op jit(solution)/shard_map/rf,rd->fd/dot_general | solution.py:441
  51.2 1.9 %multiply_reduce_fusion = (f32[512]{0:T(512)S(1)}, bf16[512,512]{1,0:T(8,128)(2,1)S(1)}, bf16[512,512]{1,0:T(8,128)(2,1)S(1)}) fusion(f32[512,512]{1,0:T(8,128)S(1)} %fusion.7, f32[512,512]{1,0:T(8,128)S(1)} %fusion.5, f32[512]{0:T(512)S(1)} %reshape.82, bf16[1,512,2048]{2,1,0:T(8,128)(2,1)S(1)} %copy-done, bf16[2,512,2048]{2,1,0:T(8,128)(2,1)S(1)} %copy-done.2), kind=kOutput, calls=%fused_computation.24 | convolution fusion | flops 1078197760 | bytes 7344128 | tf_op jit(solution)/shard_map/rd,fd->rf/dot_general | solution.py:422
  53.1 0.0 copy-start.4
  53.1 2.6 %fusion.1 = bf16[1,2048,512]{2,1,0:T(8,128)(2,1)} fusion(bf16[512,512]{1,0:T(8,128)(2,1)S(1)} %get-tuple-element.15.up_grad, bf16[2,512,2048]{2,1,0:T(8,128)(2,1)S(1)} %copy-done.2), kind=kOutput, calls=%fused_computation.4 | convolution fusion | flops 1074790400 | bytes 4718592 | tf_op jit(solution)/shard_map/rd,rf->df/dot_general | solution.py:440
  55.8 2.6 %fusion = bf16[1,2048,512]{2,1,0:T(8,128)(2,1)} fusion(bf16[512,512]{1,0:T(8,128)(2,1)S(1)} %get-tuple-element.14.gate_grad, bf16[2,512,2048]{2,1,0:T(8,128)(2,1)S(1)} %copy-done.2), kind=kOutput, calls=%fused_computation.3 | convolution fusion | flops 1074790400 | bytes 4718592 | tf_op jit(solution)/shard_map/rd,rf->df/dot_general | solution.py:439
  58.4 0.1 reshape.81
  58.5 0.6 pad.9.slot_row
  59.1 0.8 fusion.25.pick
  59.9 32.6 %combine.1 = (bf16[192,2048]{1,0:T(8,128)(2,1)}, bf16[8,512]{1,0:T(8,128)(2,1)}) custom-call(bf16[512,512]{1,0:T(8,128)(2,1)} %copy-done.4, bf16[512,512]{1,0:T(8,128)(2,1)} %copy-done.5, bf16[2048,512]{1,0:T(8,128)(2,1)} %bitcast.55, bf16[2048,512]{1,0:T(8,128)(2,1)} %bitcast.54, f32[8,1,512]{2,1,0:T(1,128)} %pad.9.slot_row, bf16[192,512]{1,0:T(8,128)(2,1)} %fusion.25.pick), custom_call_target="tpu_custom_call" | custom-call | tf_op jit(solution)/shard_map/combine/pallas_call | solution.py:343
  92.5 0.7 slice_convert_fusion.1
  93.1 0.1 reshape.83
  93.2 0.3 select_reduce_fusion.1
  93.5 0.6 pad_maximum_fusion.1
  94.1 2.1 %copy.23 = bf16[192,2048]{1,0:T(8,128)(2,1)} copy(bf16[192,2048]{1,0:T(8,128)(2,1)} %get-tuple-element.31) | data formatting | bytes 1572864
  (15 shorter events, 0.1 us)
Async XLA Ops:
  0.6 50.6 %copy-start = (bf16[1,512,2048]{2,1,0:T(8,128)(2,1)S(1)}, bf16[1,512,2048]{2,1,0:T(8,128)(2,1)}, u32[]{:S(2)}) copy-start(bf16[1,512,2048]{2,1,0:T(8,128)(2,1)} %param.13) | copy-start | bytes 6291460
  41.0 1.9 %copy-start.1 = (bf16[2,512,2048]{2,1,0:T(8,128)(2,1)}, bf16[2,512,2048]{2,1,0:T(8,128)(2,1)S(1)}, u32[]{:S(2)}) copy-start(bf16[2,512,2048]{2,1,0:T(8,128)(2,1)S(1)} %dispatch.1) | copy-start | bytes 12582916
  43.0 3.6 %copy-start.2 = (bf16[2,512,2048]{2,1,0:T(8,128)(2,1)S(1)}, bf16[2,512,2048]{2,1,0:T(8,128)(2,1)}, u32[]{:S(2)}) copy-start(bf16[2,512,2048]{2,1,0:T(8,128)(2,1)} %copy-done.1) | copy-start | bytes 12582916
  43.0 4.1 %copy-start.3 = (bf16[1,2048,512]{2,1,0:T(8,128)(2,1)S(1)}, bf16[1,2048,512]{2,1,0:T(8,128)(2,1)}, u32[]{:S(2)}) copy-start(bf16[1,2048,512]{2,1,0:T(8,128)(2,1)} %param.12) | copy-start | bytes 6291460
  53.1 2.7 %copy-start.5 = (bf16[512,512]{1,0:T(8,128)(2,1)}, bf16[512,512]{1,0:T(8,128)(2,1)S(1)}, u32[]{:S(2)}) copy-start(bf16[512,512]{1,0:T(8,128)(2,1)S(1)} %get-tuple-element.15.up_grad) | copy-start | bytes 1572868
  53.1 2.7 %copy-start.4 = (bf16[512,512]{1,0:T(8,128)(2,1)}, bf16[512,512]{1,0:T(8,128)(2,1)S(1)}, u32[]{:S(2)}) copy-start(bf16[512,512]{1,0:T(8,128)(2,1)S(1)} %get-tuple-element.14.gate_grad) | copy-start | bytes 1572868
